TPU v7x, 32 devices: a whole 2x2x4 slice. The times are simulated.
32 devices in a mesh: sp: 16 (over z, y, core), tp: 2 (over x).
Axes of the slice: x: 2, y: 2, z: 4, core: 2. Of those that a mesh axis runs over, the one named last changes fastest.
Arguments:
- tokens: bfloat16 [4096, 2048], P('sp', 'tp'), may hold values from -64 to 64
- input_norm_gain: float32 [2048], replicated, may hold values from 0.1 to 1.9
- attention_query_weight: bfloat16 [2048, 512], P(None, 'tp'), may hold values from -0.21875 to 0.21875
- attention_key_weight: bfloat16 [2048, 512], P(None, 'tp'), may hold values from -0.21875 to 0.21875
- attention_value_weight: bfloat16 [2048, 512], P(None, 'tp'), may hold values from -0.125 to 0.125
- attention_score_bias: float32 [8], P('tp'), may hold values from -18 to -7
- recurrence_query_weight: bfloat16 [2048, 1024], P(None, 'tp'), may hold values from -0.125 to 0.125
- forget_weight: bfloat16 [2048, 1024], P(None, 'tp'), may hold values from -0.125 to 0.125
- input_weight: bfloat16 [2048, 512], P(None, 'tp'), may hold values from -0.125 to 0.125
- output_gate_weight: bfloat16 [2048, 512], P(None, 'tp'), may hold values from -0.125 to 0.125
- forget_minimum: float32 [8, 128], P('tp'), may hold values from 0.9 to 1
- decay_spikes: float32 [4096, 8], P('sp', 'tp'), may hold values from -2.2 to 0
- head_norm_gain: float32 [64], replicated, may hold values from 0.1 to 1.9
- attention_output_weight: bfloat16 [512, 2048], P('tp'), may hold values from -0.25 to 0.25
- recurrence_output_weight: bfloat16 [512, 2048], P('tp'), may hold values from -0.25 to 0.25
Outputs:
- mixed: bfloat16 [4096, 2048], P('sp', 'tp')
All inputs are finite; a program needn't handle non-finite values.
Results may differ from a plain program's by a relative error of at most 0.018.
Values may be sent and summed in bfloat16 or wider, within the bound.
No kernel may reach another device: no remote copies, remote signals or barrier semaphores. Data moves between devices by JAX's collectives and lax.ppermute only.
A program may use at most 64 MiB of HBM per device.

v0:
```python
import jax
import jax.numpy as jnp
from jax import lax
from jax.sharding import PartitionSpec as P

D = 2048
HEAD = 64
REC_KEY = 128
REC_VAL = 64
KEY_SPAN = 1024
REC_SPAN = 64


epsilon = 1e-06


def entering(part, axis, combine, identity):
    place = lax.axis_index(axis)
    gathered = jax.tree.map(lambda a: lax.all_gather(a, axis), part)
    state = jax.tree.map(lambda a, e: jnp.zeros_like(a) + jnp.asarray(e, a.dtype), part, identity)

    def one(hop, state):
        return combine(
            state, jax.tree.map(lambda a: lax.dynamic_index_in_dim(a, hop, 0, False), gathered)
        )

    return lax.fori_loop(0, place, one, state)


def shards(
    tokens,
    input_norm_gain,
    attention_query_weight,
    attention_key_weight,
    attention_value_weight,
    attention_score_bias,
    recurrence_query_weight,
    forget_weight,
    input_weight,
    output_gate_weight,
    forget_minimum,
    decay_spikes,
    head_norm_gain,
    attention_output_weight,
    recurrence_output_weight,
):
    peak_value = lax.Precision.HIGHEST
    row_count = tokens.shape[0]
    weights = (
        attention_query_weight,
        attention_key_weight,
        attention_value_weight,
        recurrence_query_weight,
        forget_weight,
        input_weight,
        output_gate_weight,
    )
    values = lax.all_gather(tokens, "tp", axis=1, tiled=True).astype(jnp.float32)
    scaled = (values * input_norm_gain[None, :]).astype(jnp.bfloat16)
    partials = tuple(
        (jnp.dot(scaled, weight, preferred_element_type=jnp.float32) for weight in weights)
    )
    partials, squares = (partials, jnp.sum(values * values, axis=1))
    inverse = lax.rsqrt(squares / D + epsilon)[:, None]
    query_stick, key_stick, value_stick, query_rows, forget_rows, input_rows, gate_rows = tuple(
        ((running_total * inverse).astype(jnp.bfloat16) for running_total in partials)
    )
    position = lax.axis_index("sp")
    first_row = position * row_count
    end_row = first_row + row_count
    keys_all, values_all = (
        lax.all_gather(key_stick, "sp", axis=0, tiled=True),
        lax.all_gather(value_stick, "sp", axis=0, tiled=True),
    )
    heads_here = attention_score_bias.shape[0]
    query_heads = query_stick.reshape(row_count, heads_here, HEAD)
    query_pos = first_row + jnp.arange(row_count, dtype=jnp.int32)
    block_rows = min(KEY_SPAN, keys_all.shape[0])
    block_count = (end_row + block_rows - 1) // block_rows

    def key_block(block_number, state_carry):
        totals, carried = state_carry
        upper_row = end_row - block_number * block_rows
        lower_row = jnp.maximum(upper_row - block_rows, 0)
        key_rows = lax.dynamic_slice_in_dim(keys_all, lower_row, block_rows, 0).reshape(
            block_rows, heads_here, HEAD
        )
        value_rows = lax.dynamic_slice_in_dim(values_all, lower_row, block_rows, 0).reshape(
            block_rows, heads_here, HEAD
        )
        key_pos = lower_row + jnp.arange(block_rows, dtype=jnp.int32)
        scores = jnp.einsum(
            "qhd,khd->hqk", query_heads, key_rows, preferred_element_type=jnp.float32
        ) * HEAD ** (-0.5)
        scores = scores + attention_score_bias[:, None, None]
        before = ((key_pos[None, :] < query_pos[:, None]) & (key_pos[None, :] < upper_row))[None]
        log_rest = jnp.where(before, jax.nn.log_sigmoid(-scores), 0.0)
        later_sum = lax.cumsum(log_rest, axis=2, reverse=True) - log_rest + carried[:, :, None]
        weights_here = jnp.where(
            before, jnp.exp(jax.nn.log_sigmoid(scores) + later_sum), 0.0
        ).astype(jnp.bfloat16)
        totals = totals + jnp.einsum(
            "hqk,khd->qhd", weights_here, value_rows, preferred_element_type=jnp.float32
        )
        return (totals, carried + jnp.sum(log_rest, axis=2))

    start_carry = (
        jnp.zeros((row_count, heads_here, HEAD), jnp.float32),
        jnp.zeros((heads_here, row_count), jnp.float32),
    )
    totals, carried = lax.fori_loop(0, block_count, key_block, start_carry)
    stick_heads = totals.reshape(row_count, heads_here * HEAD).astype(jnp.bfloat16)
    state_heads_here = forget_minimum.shape[0]
    raised_values = jax.nn.silu(query_rows.astype(jnp.float32)).reshape(
        row_count, state_heads_here, REC_KEY
    )
    admitted_input = (1.0 - forget_minimum)[None] * jax.nn.sigmoid(
        -forget_rows.astype(jnp.float32).reshape(row_count, state_heads_here, REC_KEY)
    )
    forget_logarithm = jnp.log1p(-admitted_input) + decay_spikes[:, :, None]
    inputs = input_rows.astype(jnp.float32).reshape(row_count, state_heads_here, REC_VAL)
    span_count = row_count // REC_SPAN
    causal = jnp.tril(jnp.ones((REC_SPAN, REC_SPAN), jnp.bool_))[:, :, None, None]

    def to_spans(array):
        return array.reshape(span_count, REC_SPAN, state_heads_here, array.shape[-1])

    def advance(state_carry, pieces):
        recurrent_memory, offset = state_carry
        window_query, window_admitted, window_input, span_log = pieces
        running_total = jnp.cumsum(span_log, axis=0)
        log_gaps = running_total[:, None] - running_total[None, :]
        decay_table = jnp.where(causal, jnp.exp(jnp.where(causal, log_gaps, 0.0)), 0.0)
        inner_scores = jnp.einsum(
            "thk,shk,tshk->hts", window_query, window_admitted, decay_table, precision=peak_value
        )
        final_output = jnp.einsum("hts,shv->thv", inner_scores, window_input, precision=peak_value)
        final_output = final_output + jnp.einsum(
            "zbg,bgp->zbp",
            window_query * jnp.exp(running_total),
            recurrent_memory,
            precision=peak_value,
        )
        window_total = running_total[-1]
        recurrent_memory = recurrent_memory * jnp.exp(window_total)[:, :, None] + jnp.einsum(
            "rof,roi->ofi",
            window_admitted * jnp.exp(window_total[None] - running_total),
            window_input,
            precision=peak_value,
        )
        return (
            (recurrent_memory, offset + window_total),
            (final_output, running_total + offset[None]),
        )

    start_state = (
        jnp.zeros((state_heads_here, REC_KEY, REC_VAL), jnp.float32),
        jnp.zeros((state_heads_here, REC_KEY), jnp.float32),
    )
    (memory_end, offset_end), (local_out, prefix_total) = lax.scan(
        advance,
        start_state,
        (
            to_spans(raised_values),
            to_spans(admitted_input),
            to_spans(inputs),
            to_spans(forget_logarithm),
        ),
    )
    local_out = local_out.reshape(row_count, state_heads_here, REC_VAL)
    prefix_total = prefix_total.reshape(row_count, state_heads_here, REC_KEY)
    decay_all = jnp.exp(offset_end)

    def chain_combine(earlier, later_part):
        return (earlier[0] * later_part[0], earlier[1] * later_part[0][:, :, None] + later_part[1])

    identity = (jnp.ones_like(decay_all), jnp.zeros_like(memory_end))
    decay_before, incoming_state = entering((decay_all, memory_end), "sp", chain_combine, identity)
    outputs = local_out + jnp.einsum(
        "zbg,bgp->zbp", raised_values * jnp.exp(prefix_total), incoming_state, precision=peak_value
    )
    normed = (
        outputs
        * lax.rsqrt(jnp.mean(outputs * outputs, axis=2, keepdims=True) + epsilon)
        * head_norm_gain
    )
    gated_out = normed * jax.nn.silu(
        gate_rows.astype(jnp.float32).reshape(row_count, state_heads_here, REC_VAL)
    )
    recurrence_heads = gated_out.reshape(row_count, state_heads_here * REC_VAL).astype(jnp.bfloat16)
    stick_all, state_all = (
        lax.all_gather(stick_heads, "tp", axis=1, tiled=True),
        lax.all_gather(recurrence_heads, "tp", axis=1, tiled=True),
    )
    stick_columns, state_columns = (
        lax.all_to_all(attention_output_weight, "tp", split_axis=1, concat_axis=0, tiled=True),
        lax.all_to_all(recurrence_output_weight, "tp", split_axis=1, concat_axis=0, tiled=True),
    )
    mixed_out = jnp.dot(stick_all, stick_columns, preferred_element_type=jnp.float32)
    mixed_out = (
        mixed_out + jnp.dot(state_all, state_columns, preferred_element_type=jnp.float32)
    ).astype(jnp.bfloat16)
    return mixed_out


def solution(mesh):
    placed = (
        P("sp", "tp"),
        P(),
        P(None, "tp"),
        P(None, "tp"),
        P(None, "tp"),
        P("tp"),
        P(None, "tp"),
        P(None, "tp"),
        P(None, "tp"),
        P(None, "tp"),
        P("tp", None),
        P("sp", "tp"),
        P(),
        P("tp", None),
        P("tp", None),
    )
    return jax.shard_map(
        shards, mesh=mesh, in_specs=placed, out_specs=P("sp", "tp"), check_vma=False
    )
```

profile of v0, /device:TPU:24, one launch (start us, length us, event | category | flops | bytes accessed | tf_op | source)
XLA Modules:
  0.0 392.3 jit_solution(10254816213094781945)
XLA Ops:
  8.9 22.3 %all-gather.8.cloned.1.call-done = bf16[256,2048]{1,0:T(8,128)(2,1)} async-done(((bf16[256,1024]{1,0:T(8,128)(2,1)}), bf16[256,2048]{1,0:T(8,128)(2,1)}) %all-gather.8.cloned.1.call-update) | async-done | bytes 1048592 | tf_op jit(solution)/shard_map/all_gather | solution.py:58
  43.7 79.1 %while.47 = (s32[]{:T(128)}, f32[4,128,64]{1,2,0:T(8,128)S(1)}, f32[4,128]{1,0:T(4,128)S(1)}, f32[4,64,4,64]{1,0,3,2:T(4,128)}, f32[4,64,4,128]{3,2,1,0:T(4,128)...) while((s32[]{:T(128)}, f32[4,128,64]{1,2,0:T(8,128)S(1)}, ...), condition=%wide.region_8.9_spmd.clone.clone, body=%wide.region_6.8_spmd.clone.clone.sunk | while | flops 77829120 | bytes 20935308 | solution.py:160
  44.4 5.9 %select_bitcast_fusion.2 = f32[4,64,64,128]{3,0,2,1:T(4,128)S(1)} fusion(f32[64,4,128]{2,1,0:T(4,128)S(1)} %fusion.122, pred[64,64]{1,0:T(8,128)(4,1)S(1)} %fusion.124), kind=kLoop, calls=%fused_computation.39.clone.1 | loop fusion | flops 6291456 | bytes 8523776 | tf_op jit(solution)/shard_map/while
  50.4 7.4 %fusion.125 = f32[4,64,64]{1,2,0:T(8,128)S(1)} fusion(f32[4,64,64,128]{3,0,2,1:T(4,128)S(1)} %select_bitcast_fusion.2, f32[4,128,64]{1,2,0:T(8,128)S(1)} %copy.196, f32[4,128,64]{1,2,0:T(8,128)S(1)} %copy.197), kind=kLoop, calls=%fused_computation.38.clone.1 | loop fusion | flops 6275072 | bytes 8716288 | tf_op jit(solution)/shard_map/while/body/eval_jaxpr/thk,shk,tshk->hts/dot_general | solution.py:134
  64.1 5.9 %select_bitcast_fusion.2 = f32[4,64,64,128]{3,0,2,1:T(4,128)S(1)} fusion(f32[64,4,128]{2,1,0:T(4,128)S(1)} %fusion.122, pred[64,64]{1,0:T(8,128)(4,1)S(1)} %fusion.124), kind=kLoop, calls=%fused_computation.39.clone.1 | loop fusion | flops 6291456 | bytes 8523776 | tf_op jit(solution)/shard_map/while
  70.1 7.4 %fusion.125 = f32[4,64,64]{1,2,0:T(8,128)S(1)} fusion(f32[4,64,64,128]{3,0,2,1:T(4,128)S(1)} %select_bitcast_fusion.2, f32[4,128,64]{1,2,0:T(8,128)S(1)} %copy.196, f32[4,128,64]{1,2,0:T(8,128)S(1)} %copy.197), kind=kLoop, calls=%fused_computation.38.clone.1 | loop fusion | flops 6275072 | bytes 8716288 | tf_op jit(solution)/shard_map/while/body/eval_jaxpr/thk,shk,tshk->hts/dot_general | solution.py:134
  77.9 4.5 %dynamic_update_slice.16 = f32[4,64,4,64]{1,0,3,2:T(4,128)} dynamic-update-slice(f32[4,64,4,64]{1,0,3,2:T(4,128)} %get-tuple-element.737, f32[1,64,4,64]{1,0,3,2:T(1,128)S(1)} %bitcast.197, s32[]{:T(128)} %get-tuple-element.734, s32[]{:T(128)} %constant.115.clone.1..sunk.2, s32[]{:T(128)} %constant.115.clone.1..sunk.2, s32[]{:T(128)} %constant.115.clone.1..sunk.2) | dynamic-update-slice | bytes 131076 | tf_op jit(solution)/shard_map/while/body/jit(dynamic_update_index_in_dim)/dynamic_update_slice | solution.py:160
  83.8 5.9 %select_bitcast_fusion.2 = f32[4,64,64,128]{3,0,2,1:T(4,128)S(1)} fusion(f32[64,4,128]{2,1,0:T(4,128)S(1)} %fusion.122, pred[64,64]{1,0:T(8,128)(4,1)S(1)} %fusion.124), kind=kLoop, calls=%fused_computation.39.clone.1 | loop fusion | flops 6291456 | bytes 8523776 | tf_op jit(solution)/shard_map/while
  89.8 7.4 %fusion.125 = f32[4,64,64]{1,2,0:T(8,128)S(1)} fusion(f32[4,64,64,128]{3,0,2,1:T(4,128)S(1)} %select_bitcast_fusion.2, f32[4,128,64]{1,2,0:T(8,128)S(1)} %copy.196, f32[4,128,64]{1,2,0:T(8,128)S(1)} %copy.197), kind=kLoop, calls=%fused_computation.38.clone.1 | loop fusion | flops 6275072 | bytes 8716288 | tf_op jit(solution)/shard_map/while/body/eval_jaxpr/thk,shk,tshk->hts/dot_general | solution.py:134
  103.6 5.9 %select_bitcast_fusion.2 = f32[4,64,64,128]{3,0,2,1:T(4,128)S(1)} fusion(f32[64,4,128]{2,1,0:T(4,128)S(1)} %fusion.122, pred[64,64]{1,0:T(8,128)(4,1)S(1)} %fusion.124), kind=kLoop, calls=%fused_computation.39.clone.1 | loop fusion | flops 6291456 | bytes 8523776 | tf_op jit(solution)/shard_map/while
  109.5 7.4 %fusion.125 = f32[4,64,64]{1,2,0:T(8,128)S(1)} fusion(f32[4,64,64,128]{3,0,2,1:T(4,128)S(1)} %select_bitcast_fusion.2, f32[4,128,64]{1,2,0:T(8,128)S(1)} %copy.196, f32[4,128,64]{1,2,0:T(8,128)S(1)} %copy.197), kind=kLoop, calls=%fused_computation.38.clone.1 | loop fusion | flops 6275072 | bytes 8716288 | tf_op jit(solution)/shard_map/while/body/eval_jaxpr/thk,shk,tshk->hts/dot_general | solution.py:134
  117.3 4.5 %dynamic_update_slice.16 = f32[4,64,4,64]{1,0,3,2:T(4,128)} dynamic-update-slice(f32[4,64,4,64]{1,0,3,2:T(4,128)} %get-tuple-element.737, f32[1,64,4,64]{1,0,3,2:T(1,128)S(1)} %bitcast.197, s32[]{:T(128)} %get-tuple-element.734, s32[]{:T(128)} %constant.115.clone.1..sunk.2, s32[]{:T(128)} %constant.115.clone.1..sunk.2, s32[]{:T(128)} %constant.115.clone.1..sunk.2) | dynamic-update-slice | bytes 131076 | tf_op jit(solution)/shard_map/while/body/jit(dynamic_update_index_in_dim)/dynamic_update_slice | solution.py:160
  133.4 12.4 %all-to-all-done = bf16[256,2,1024]{0,2,1:T(8,128)(2,1)S(1)} async-done(((bf16[256,2,1024]{0,2,1:T(8,128)(2,1)}), bf16[256,2,1024]{0,2,1:T(8,128)(2,1)S(1)}, u32[]{:S(2)}, u32[]{:S(2)}) %all-to-all-start) | async-done | bytes 1048608 | tf_op jit(solution)/shard_map/all_to_all | solution.py:196
  153.4 8.9 %all-to-all-done.1 = bf16[256,2,1024]{0,2,1:T(8,128)(2,1)S(1)} async-done(((bf16[256,2,1024]{0,2,1:T(8,128)(2,1)}), bf16[256,2,1024]{0,2,1:T(8,128)(2,1)S(1)}, u32[]{:S(2)}, u32[]{:S(2)}) %all-to-all-start.1) | async-done | bytes 1048608 | tf_op jit(solution)/shard_map/all_to_all | solution.py:197
  169.7 17.1 %all-gather.2 = f32[16,4,128]{2,1,0:T(4,128)S(1)} all-gather(f32[1,4,128]{2,1,0:T(4,128)S(1)} %exponential_bitcast_fusion), channel_id=2, replica_groups=mesh['sp'=16,'tp'=2] {'sp'}, dimensions={0}, use_global_device_ids=true | all-gather | bytes 34816 | tf_op jit(solution)/shard_map/all_gather | solution.py:19
  186.9 15.2 %while.45 = (s32[]{:T(128)}, f32[4,128,64]{2,1,0:T(8,128)S(1)}, s32[]{:T(128)}, f32[16,4,128]{2,1,0:T(4,128)S(1)}, f32[16,4,128,64]{2,3,1,0:T(8,128)}, /*index=5*/s32[]{:T(128)}, s32[]{:T(128)}, s32[]{:T(128)}) while((s32[]{:T(128)}, f32[4,128,64]{2,1,0:T(8,128)S(1)}, s32[]{:T(128)}, f32[16,4,128]{2,1,0:T(4,128)S(1)}, ...), condition=%wide.region_10.11_spmd, body=%wide.region_9.10_spmd.sunk | while | flops 65541 | bytes 923775 | solution.py:27
  203.0 6.5 %all_gather.35 = bf16[256,512]{0,1:T(8,128)(2,1)} all-gather(bf16[256,256]{0,1:T(8,128)(2,1)S(1)} %bitcast.205), channel_id=1, replica_groups=mesh['sp'=16,'tp'=2] {'tp'}, dimensions={1}, use_global_device_ids=true | all-gather | bytes 393216 | tf_op jit(solution)/shard_map/all_gather | solution.py:193
  209.5 38.9 %all-gather.12.cloned.1.call-done = bf16[4096,256]{1,0:T(8,128)(2,1)} async-done(((bf16[256,256]{1,0:T(8,128)(2,1)}), bf16[4096,256]{1,0:T(8,128)(2,1)}) %all-gather.12.cloned.1.call-update) | async-done | bytes 2097168 | tf_op jit(solution)/shard_map/all_gather | solution.py:72
  248.4 126.6 %while.46 = (s32[]{:T(128)}, f32[256,4,64]{0,2,1:T(8,128)S(1)}, f32[4,256]{1,0:T(4,128)S(1)}, s32[]{:T(128)}, s32[]{:T(128)}, /*index=5*/bf16[4096,256]{1,0:T(8,...) while((s32[]{:T(128)}, f32[256,4,64]{0,2,1:T(8,128)S(1)}, ...), condition=%wide.region_5.6_spmd.clone, body=%wide.region_1.5_spmd.clone.sunk | while | flops 438962432 | bytes 86642984 | solution.py:111
  250.5 5.3 %fusion.111 = (f32[4,256]{1,0:T(4,128)S(1)}, f32[4,256,1024]{1,2,0:T(8,128)S(1)}, f32[4,1024,256]{2,1,0:T(8,128)}) fusion(f32[4]{0:T(128)S(1)} %get-tuple-element.716, pred[256,1024]{0,1:T(8,128)(4,1)S(1)} %compare_and_fusion.2, bf16[1024,4,64]{0,2,1:T(8,128)(2,1)S(1)} %bitcast.196, bf16[256,4,64]{0,2,1:T(8,128)(2,1)S(1)} %get-tuple-element.715), kind=kOutput, calls=%fused_computation.36.clone.1 | convolution fusion | flops 145751040 | bytes 9310224 | tf_op jit(solution)/shard_map/while/body/qhd,khd->hqk/dot_general | solution.py:92
  255.8 10.1 %fusion.112 = f32[4,256,8,128]{1,2,3,0:T(8,128)S(1)} fusion(f32[4,256,8,128]{1,3,2,0:T(8,128)S(1)} %bitcast.194), kind=kOutput, calls=%fused_computation.23.clone.1 | output fusion | flops 133169152 | bytes 8388608 | tf_op jit(solution)/shard_map/reduce-window.6
  272.7 6.6 %fusion.113 = bf16[4,256,1024]{1,2,0:T(8,128)(2,1)S(1)} fusion(f32[4,256,8,128]{1,3,2,0:T(8,128)S(1)} %copy.191, f32[4,1024,256]{2,1,0:T(8,128)S(1)} %copy-done.3, f32[4,256]{1,0:T(4,128)S(1)} %get-tuple-element.695, f32[4]{0:T(128)S(1)} %get-tuple-element.716, pred[256,1024]{0,1:T(8,128)(4,1)S(1)} %compare_and_fusion.2), kind=kLoop, calls=%fused_computation.11.clone.1 | loop fusion | flops 24117248 | bytes 10752016 | tf_op jit(solution)/shard_map/while/body/convert_element_type | solution.py:101
  282.1 5.3 %fusion.111 = (f32[4,256]{1,0:T(4,128)S(1)}, f32[4,256,1024]{1,2,0:T(8,128)S(1)}, f32[4,1024,256]{2,1,0:T(8,128)}) fusion(f32[4]{0:T(128)S(1)} %get-tuple-element.716, pred[256,1024]{0,1:T(8,128)(4,1)S(1)} %compare_and_fusion.2, bf16[1024,4,64]{0,2,1:T(8,128)(2,1)S(1)} %bitcast.196, bf16[256,4,64]{0,2,1:T(8,128)(2,1)S(1)} %get-tuple-element.715), kind=kOutput, calls=%fused_computation.36.clone.1 | convolution fusion | flops 145751040 | bytes 9310224 | tf_op jit(solution)/shard_map/while/body/qhd,khd->hqk/dot_general | solution.py:92
  287.4 10.1 %fusion.112 = f32[4,256,8,128]{1,2,3,0:T(8,128)S(1)} fusion(f32[4,256,8,128]{1,3,2,0:T(8,128)S(1)} %bitcast.194), kind=kOutput, calls=%fused_computation.23.clone.1 | output fusion | flops 133169152 | bytes 8388608 | tf_op jit(solution)/shard_map/reduce-window.6
  304.4 6.6 %fusion.113 = bf16[4,256,1024]{1,2,0:T(8,128)(2,1)S(1)} fusion(f32[4,256,8,128]{1,3,2,0:T(8,128)S(1)} %copy.191, f32[4,1024,256]{2,1,0:T(8,128)S(1)} %copy-done.3, f32[4,256]{1,0:T(4,128)S(1)} %get-tuple-element.695, f32[4]{0:T(128)S(1)} %get-tuple-element.716, pred[256,1024]{0,1:T(8,128)(4,1)S(1)} %compare_and_fusion.2), kind=kLoop, calls=%fused_computation.11.clone.1 | loop fusion | flops 24117248 | bytes 10752016 | tf_op jit(solution)/shard_map/while/body/convert_element_type | solution.py:101
  313.8 5.3 %fusion.111 = (f32[4,256]{1,0:T(4,128)S(1)}, f32[4,256,1024]{1,2,0:T(8,128)S(1)}, f32[4,1024,256]{2,1,0:T(8,128)}) fusion(f32[4]{0:T(128)S(1)} %get-tuple-element.716, pred[256,1024]{0,1:T(8,128)(4,1)S(1)} %compare_and_fusion.2, bf16[1024,4,64]{0,2,1:T(8,128)(2,1)S(1)} %bitcast.196, bf16[256,4,64]{0,2,1:T(8,128)(2,1)S(1)} %get-tuple-element.715), kind=kOutput, calls=%fused_computation.36.clone.1 | convolution fusion | flops 145751040 | bytes 9310224 | tf_op jit(solution)/shard_map/while/body/qhd,khd->hqk/dot_general | solution.py:92
  319.1 10.1 %fusion.112 = f32[4,256,8,128]{1,2,3,0:T(8,128)S(1)} fusion(f32[4,256,8,128]{1,3,2,0:T(8,128)S(1)} %bitcast.194), kind=kOutput, calls=%fused_computation.23.clone.1 | output fusion | flops 133169152 | bytes 8388608 | tf_op jit(solution)/shard_map/reduce-window.6
  336.0 6.6 %fusion.113 = bf16[4,256,1024]{1,2,0:T(8,128)(2,1)S(1)} fusion(f32[4,256,8,128]{1,3,2,0:T(8,128)S(1)} %copy.191, f32[4,1024,256]{2,1,0:T(8,128)S(1)} %copy-done.3, f32[4,256]{1,0:T(4,128)S(1)} %get-tuple-element.695, f32[4]{0:T(128)S(1)} %get-tuple-element.716, pred[256,1024]{0,1:T(8,128)(4,1)S(1)} %compare_and_fusion.2), kind=kLoop, calls=%fused_computation.11.clone.1 | loop fusion | flops 24117248 | bytes 10752016 | tf_op jit(solution)/shard_map/while/body/convert_element_type | solution.py:101
  345.4 5.3 %fusion.111 = (f32[4,256]{1,0:T(4,128)S(1)}, f32[4,256,1024]{1,2,0:T(8,128)S(1)}, f32[4,1024,256]{2,1,0:T(8,128)}) fusion(f32[4]{0:T(128)S(1)} %get-tuple-element.716, pred[256,1024]{0,1:T(8,128)(4,1)S(1)} %compare_and_fusion.2, bf16[1024,4,64]{0,2,1:T(8,128)(2,1)S(1)} %bitcast.196, bf16[256,4,64]{0,2,1:T(8,128)(2,1)S(1)} %get-tuple-element.715), kind=kOutput, calls=%fused_computation.36.clone.1 | convolution fusion | flops 145751040 | bytes 9310224 | tf_op jit(solution)/shard_map/while/body/qhd,khd->hqk/dot_general | solution.py:92
  350.7 10.1 %fusion.112 = f32[4,256,8,128]{1,2,3,0:T(8,128)S(1)} fusion(f32[4,256,8,128]{1,3,2,0:T(8,128)S(1)} %bitcast.194), kind=kOutput, calls=%fused_computation.23.clone.1 | output fusion | flops 133169152 | bytes 8388608 | tf_op jit(solution)/shard_map/reduce-window.6
  367.7 6.6 %fusion.113 = bf16[4,256,1024]{1,2,0:T(8,128)(2,1)S(1)} fusion(f32[4,256,8,128]{1,3,2,0:T(8,128)S(1)} %copy.191, f32[4,1024,256]{2,1,0:T(8,128)S(1)} %copy-done.3, f32[4,256]{1,0:T(4,128)S(1)} %get-tuple-element.695, f32[4]{0:T(128)S(1)} %get-tuple-element.716, pred[256,1024]{0,1:T(8,128)(4,1)S(1)} %compare_and_fusion.2), kind=kLoop, calls=%fused_computation.11.clone.1 | loop fusion | flops 24117248 | bytes 10752016 | tf_op jit(solution)/shard_map/while/body/convert_element_type | solution.py:101
  375.1 6.4 %all_gather.30 = bf16[256,512]{0,1:T(8,128)(2,1)S(1)} all-gather(bf16[256,256]{0,1:T(8,128)(2,1)S(1)} %bitcast.204), channel_id=1, replica_groups=mesh['sp'=16,'tp'=2] {'tp'}, dimensions={1}, use_global_device_ids=true | all-gather | bytes 393216 | tf_op jit(solution)/shard_map/all_gather | solution.py:192
  (249 shorter events, 115.0 us)
Async XLA Ops:
  6.5 26.2 %copy-start = (bf16[2048,512]{1,0:T(8,128)(2,1)S(1)}, bf16[2048,512]{1,0:T(8,128)(2,1)}, u32[]{:S(2)}) copy-start(bf16[2048,512]{1,0:T(8,128)(2,1)} %param.28) | copy-start | bytes 6291460
  6.5 24.6 %all-gather.8.cloned.1.call-start = ((), (), s32[]{:S(2)}) async-start(), calls=%async_computation.2 | async-start | bytes 1572864 | tf_op jit(solution)/shard_map/all_gather | solution.py:58
  7.3 179.6 %all-gather.14.cloned.1.call-start = ((), (), s32[]{:S(2)}) async-start(), calls=%async_computation.5 | async-start | bytes 2228224 | tf_op jit(solution)/shard_map/all_gather | solution.py:19
  8.2 29.5 %copy-start.12 = (f32[2048]{0:T(1024)S(1)}, f32[2048]{0:T(1024)}, u32[]{:S(2)}) copy-start(f32[2048]{0:T(1024)} %param.22) | copy-start | bytes 24580
  31.2 6.5 %copy-start.7 = (bf16[256,2048]{1,0:T(8,128)(2,1)S(1)}, bf16[256,2048]{1,0:T(8,128)(2,1)}, u32[]{:S(2)}) copy-start(bf16[256,2048]{1,0:T(8,128)(2,1)} %all-gather.8.cloned.1.call-done) | copy-start | bytes 3145732
  40.0 3.6 copy-start.5
  122.7 0.7 copy-start.4
  122.7 9.4 %copy-start.9 = (bf16[256,2048]{1,0:T(8,128)(2,1)S(1)}, bf16[256,2048]{1,0:T(8,128)(2,1)}, u32[]{:S(2)}) copy-start(bf16[256,2048]{1,0:T(8,128)(2,1)} %param.35) | copy-start | bytes 3145732
  123.4 86.1 %all-gather.10.cloned.1.call-start = ((), (), s32[]{:S(2)}) async-start(), calls=%async_computation.3 | async-start | bytes 2228224 | tf_op jit(solution)/shard_map/all_gather | solution.py:73
  126.1 23.3 %copy-start.8 = (bf16[256,2048]{1,0:T(8,128)(2,1)S(1)}, bf16[256,2048]{1,0:T(8,128)(2,1)}, u32[]{:S(2)}) copy-start(bf16[256,2048]{1,0:T(8,128)(2,1)} %all-gather.8.cloned.1.call-done) | copy-start | bytes 3145732
  128.5 17.3 %all-to-all-start = ((bf16[256,2,1024]{0,2,1:T(8,128)(2,1)}), bf16[256,2,1024]{0,2,1:T(8,128)(2,1)S(1)}, u32[]{:S(2)}, u32[]{:S(2)}) async-start(bf16[256,2,1024]{0,2,1:T(8,128)(2,1)} %bitcast.6), calls=%async_computation | async-start | bytes 2097152 | tf_op jit(solution)/shard_map/all_to_all | solution.py:196
  145.8 16.4 %all-to-all-start.1 = ((bf16[256,2,1024]{0,2,1:T(8,128)(2,1)}), bf16[256,2,1024]{0,2,1:T(8,128)(2,1)S(1)}, u32[]{:S(2)}, u32[]{:S(2)}) async-start(bf16[256,2,1024]{0,2,1:T(8,128)(2,1)} %bitcast.16), calls=%async_computation.1 | async-start | bytes 2097152 | tf_op jit(solution)/shard_map/all_to_all | solution.py:197
  149.4 99.0 %all-gather.12.cloned.1.call-start = ((), (), s32[]{:S(2)}) async-start(), calls=%async_computation.4 | async-start | bytes 2228224 | tf_op jit(solution)/shard_map/all_gather | solution.py:72
  169.6 32.5 %copy-start.6 = (f32[256,512]{1,0:T(8,128)S(1)}, f32[256,512]{1,0:T(8,128)}, u32[]{:S(2)}) copy-start(f32[256,512]{1,0:T(8,128)} %copy-done.5) | copy-start | bytes 1572868
  186.8 16.0 %copy-start.11 = (f32[64]{0:T(128)S(1)}, f32[64]{0:T(128)}, u32[]{:S(2)}) copy-start(f32[64]{0:T(128)} %param.33) | copy-start | bytes 772
  186.9 61.5 %copy-start.10 = (f32[4]{0:T(128)S(1)}, f32[4]{0:T(128)}, u32[]{:S(2)}) copy-start(f32[4]{0:T(128)} %param.26) | copy-start | bytes 52
  265.8 2.0 copy-start.2
  270.5 2.2 copy-start.3
  297.5 2.0 copy-start.2
  302.2 2.2 copy-start.3
  329.1 2.0 copy-start.2
  333.8 2.2 copy-start.3
  360.8 2.0 copy-start.2
  365.5 2.2 copy-start.3
  375.0 10.7 %copy-start.1 = (bf16[2048,512]{1,0:T(8,128)(2,1)S(1)}, bf16[2048,512]{1,0:T(8,128)(2,1)}, u32[]{:S(2)}) copy-start(bf16[2048,512]{1,0:T(8,128)(2,1)} %param.28) | copy-start | bytes 6291460
Sparse Core Ops, SparseCore 0:
  8.9 22.2 all-gather.7
  123.5 40.1 all-gather.13
  165.9 40.2 all-gather.9
  208.2 40.1 all-gather.11
where the time goes:
time: 394 us; the launch traced here: 392 us
  other arithmetic  141 us (36%)
  waiting for transfers between devices  83.2 us (21%)
  local copies, waits for them, and re-layouts  68.8 us (17%)
  matrix products  46.7 us (12%)
  blocking collectives  30 us (8%)
  between operations  13.4 us (3%)
  starting transfers between devices  7.29 us (2%)
    another operation x8, other arithmetic  40.6 us
    all_gather x1, waiting for transfers between devices, shards(): lax.all_gather(key_stick, 'sp', axis=0, tiled=True)  38.9 us
    dot_general x4, other arithmetic, advance(): jnp.einsum('thk,shk,tshk->hts', window_query, window_admitted, decay_tabl...  29.4 us
    convert_element_type x4, other arithmetic, key_block(): weights_here = jnp.where(before, jnp.exp(jax.nn.log_sigmoid(scores) + lat...  26.4 us
    while x4, other arithmetic  23.6 us
    all_gather x1, waiting for transfers between devices, shards(): lax.all_gather(tokens, 'tp', axis=1, tiled=True).astype(jnp.float32)  22.3 us
    dot_general x4, matrix products, key_block(): jnp.einsum('qhd,khd->hqk', query_heads, key_rows, preferred_element_type=...  21.1 us
    dynamic_update_slice x4, local copies, waits for them, and re-layouts, shards(): lax.scan(advance, start_state, (to_spans(raised_values), to_spans(admitte...  17.9 us
  transfers between devices with their start and end apart: 6, of which 4 were waited for; matrix products, arithmetic and copies ran while one was open for 9% of the time, Pallas kernels for 0%

commit v1 on v0

v1 whole, which is shorter than its diff:
```python
import jax
import jax.numpy as jnp
from jax import lax
from jax.experimental import pallas as pl
from jax.experimental.pallas import tpu as pltpu
from jax.sharding import PartitionSpec as P

HEAD = 64
REC_KEY = 128
REC_VAL = 64
LANES = 128
STATE_ROWS = 72
epsilon = 1e-06
F32 = jnp.float32
BF16 = jnp.bfloat16
EXACT = lax.Precision.HIGHEST


def dot(a, b, dims=((1,), (0,)), precision=None):
    return lax.dot_general(a, b, (dims, ((), ())), precision=precision, preferred_element_type=F32)


def tri(n, compare):
    row = lax.broadcasted_iota(jnp.int32, (n, n), 0)
    col = lax.broadcasted_iota(jnp.int32, (n, n), 1)
    return compare(row, col)


def project(tokens, gain, weights):
    rows, width = tokens.shape
    step = 256
    steps = width // step
    cols = [w.shape[1] for w in weights]

    def body(x_ref, g_ref, *refs):
        w_refs = refs[:7]
        q_ref, kv_ref, rq_ref, rf_ref, ri_ref, rg_ref = refs[7:13]
        accs = refs[13:20]
        sq_ref = refs[20]
        i = pl.program_id(0)
        x = x_ref[...].astype(F32)
        scaled = (x * g_ref[...]).astype(BF16)
        squares = jnp.sum(x * x, axis=1, keepdims=True)

        @pl.when(i == 0)
        def _():
            sq_ref[...] = squares
            for acc, w in zip(accs, w_refs):
                acc[...] = dot(scaled, w[...])

        @pl.when(i > 0)
        def _():
            sq_ref[...] += squares
            for acc, w in zip(accs, w_refs):
                acc[...] += dot(scaled, w[...])

        @pl.when(i == steps - 1)
        def _():
            inverse = lax.rsqrt(sq_ref[...] / width + epsilon)
            done = [(acc[...] * inverse).astype(BF16) for acc in accs]
            q_ref[...] = done[0]
            kv_ref[:, : cols[1]] = done[1]
            kv_ref[:, cols[1] :] = done[2]
            rq_ref[...] = done[3]
            rf_ref[...] = done[4]
            ri_ref[...] = done[5]
            rg_ref[...] = done[6]

    outs = [cols[0], cols[1] + cols[2], *cols[3:]]
    return pl.pallas_call(
        body,
        grid=(steps,),
        in_specs=[
            pl.BlockSpec((rows, step), lambda i: (0, i)),
            pl.BlockSpec((1, step), lambda i: (0, i)),
            *[pl.BlockSpec((step, c), lambda i: (i, 0)) for c in cols],
        ],
        out_specs=[pl.BlockSpec((rows, c), lambda i: (0, 0)) for c in outs],
        out_shape=[jax.ShapeDtypeStruct((rows, c), BF16) for c in outs],
        scratch_shapes=[pltpu.VMEM((rows, c), F32) for c in cols] + [pltpu.VMEM((rows, 1), F32)],
        name="project",
    )(tokens, gain[None, :], *weights)


def stick(place, bias, query, keys_values):
    rows, width = query.shape
    total = keys_values.shape[0]
    slab = min(LANES, width)
    slabs = width // slab
    per = slab // HEAD
    if slab % LANES == 0:
        keys, values, shift = keys_values, keys_values, slabs
    else:
        keys, values, shift = keys_values[:, :width], keys_values[:, width:], 0

    def body(place_ref, bias_ref, q_ref, k_ref, v_ref, o_ref, acc_ref, carry_ref, tri_ref):
        p = pl.program_id(0)
        here = place_ref[0]
        lane = lax.broadcasted_iota(jnp.int32, (rows, slab), 1) // HEAD
        scaled = q_ref[...] * jnp.asarray(HEAD**-0.5, BF16)
        heads = [jnp.where(lane == h, scaled, jnp.zeros_like(scaled)) for h in range(per)]
        tri_ref[...] = jnp.where(tri(rows, lambda r, c: r > c), 1.0, 0.0).astype(BF16)

        def block(number, diagonal):
            start = pl.multiple_of(number * rows, rows)
            key = k_ref[pl.ds(start, rows), :]
            value = v_ref[pl.ds(start, rows), :]
            for h in range(per):
                score = dot(heads[h], key, ((1,), (1,))) + bias_ref[p * per + h]
                small = jnp.log(1.0 + jnp.exp(-jnp.abs(score)))
                rest = jnp.maximum(score, 0.0) + small
                take = jnp.minimum(score, 0.0) - small
                if diagonal:
                    before = tri(rows, lambda r, c: c < r)
                    rest = jnp.where(before, rest, 0.0)
                later = dot(rest.astype(BF16), tri_ref[...])
                gone = later[:, 0:1] + rest[:, 0:1]
                if diagonal:
                    weight = jnp.where(before, jnp.exp(take - later), 0.0)
                else:
                    weight = jnp.exp(take - later - carry_ref[h])
                part = jnp.where(lane == h, dot(weight.astype(BF16), value), 0.0)
                if diagonal and h == 0:
                    acc_ref[...] = part
                else:
                    acc_ref[...] += part
                if diagonal:
                    carry_ref[h] = gone
                else:
                    carry_ref[h] += gone

        block(here, True)

        @pl.loop(0, here)
        def _(i):
            block(here - 1 - i, False)

        o_ref[...] = acc_ref[...].astype(BF16)

    return pl.pallas_call(
        body,
        grid=(slabs,),
        in_specs=[
            pl.BlockSpec(memory_space=pltpu.SMEM),
            pl.BlockSpec(memory_space=pltpu.SMEM),
            pl.BlockSpec((rows, slab), lambda p: (0, p)),
            pl.BlockSpec((total, slab), lambda p: (0, p)),
            pl.BlockSpec((total, slab), lambda p: (0, shift + p)),
        ],
        out_specs=pl.BlockSpec((rows, slab), lambda p: (0, p)),
        out_shape=jax.ShapeDtypeStruct((rows, width), BF16),
        scratch_shapes=[
            pltpu.VMEM((rows, slab), F32),
            pltpu.VMEM((per, rows, 1), F32),
            pltpu.VMEM((rows, rows), BF16),
        ],
        name="stick",
    )(place, bias, query, keys, values)


def local_recurrence(query, forget, inputs, minimum, spikes):
    rows = query.shape[0]
    heads = minimum.shape[0]
    width = heads * REC_VAL
    slab = min(LANES, width)
    per = slab // REC_VAL

    def body(q_ref, f_ref, x_ref, m_ref, s_ref, st_ref, raw_ref, qd_ref, state_ref):
        causal = tri(rows, lambda r, c: c <= r)
        lower = jnp.where(causal, 1.0, 0.0)
        spike_col = dot(lower, s_ref[...], precision=EXACT)
        spike_row = dot(st_ref[...], lower, ((1,), (1,)), precision=EXACT)
        lane = lax.broadcasted_iota(jnp.int32, (rows, slab), 1) // REC_VAL
        for p in range(width // slab):
            x = x_ref[:, p * slab : (p + 1) * slab]
            raw = None
            for hh in range(per):
                h = p * per + hh
                keys = slice(h * REC_KEY, (h + 1) * REC_KEY)
                q = q_ref[:, keys].astype(F32)
                lifted = q * jax.nn.sigmoid(q)
                intake = (1.0 - m_ref[h : h + 1, :]) * jax.nn.sigmoid(-f_ref[:, keys].astype(F32))
                gap = dot(lower, jnp.log1p(-intake), precision=EXACT)
                middle = gap[rows // 2 : rows // 2 + 1, :]
                column = spike_col[:, h : h + 1]
                across = spike_row[h : h + 1, :]
                up = (lifted * jnp.exp(gap - middle)).astype(BF16)
                down = (intake * jnp.exp(middle - gap)).astype(BF16)
                table = jnp.where(causal, jnp.exp(jnp.minimum(column - across, 0.0)), 0.0)
                inner = dot(up, down, ((1,), (1,)))
                inner = (jnp.where(causal, inner, 0.0) * table).astype(BF16)
                own = jnp.where(lane == hh, x, jnp.zeros_like(x))
                part = dot(inner, own)
                raw = part if raw is None else raw + part
                whole = gap + column
                last = whole[rows - 1 : rows, :]
                qd_ref[:, keys] = (lifted * jnp.exp(whole)).astype(BF16)
                leaving = (intake * jnp.exp(last - whole)).astype(BF16)
                memory = dot(x, leaving, ((0,), (0,)))
                state_ref[h, :REC_VAL, :] = memory[hh * REC_VAL : (hh + 1) * REC_VAL, :]
                state_ref[h, REC_VAL:, :] = jnp.broadcast_to(
                    jnp.exp(last), (STATE_ROWS - REC_VAL, REC_KEY)
                )
            raw_ref[:, p * slab : (p + 1) * slab] = raw

    return pl.pallas_call(
        body,
        out_shape=[
            jax.ShapeDtypeStruct((rows, width), F32),
            jax.ShapeDtypeStruct((rows, heads * REC_KEY), BF16),
            jax.ShapeDtypeStruct((heads, STATE_ROWS, REC_KEY), F32),
        ],
        name="local_recurrence",
    )(query, forget, inputs, minimum, spikes, spikes.T)


def finish_recurrence(place, raw, decayed, states, gate, gain):
    rows, width = raw.shape
    heads = width // REC_VAL
    slab = min(LANES, width)
    per = slab // REC_VAL

    def body(place_ref, raw_ref, qd_ref, st_ref, g_ref, n_ref, o_ref, s_ref):
        s_ref[...] = jnp.zeros_like(s_ref)

        @pl.loop(0, place_ref[0])
        def _(j):
            for h in range(heads):
                s_ref[h] = s_ref[h] * st_ref[j, h, REC_VAL : REC_VAL + 1, :] + st_ref[j, h, :REC_VAL, :]

        lane = lax.broadcasted_iota(jnp.int32, (rows, slab), 1) // REC_VAL
        for p in range(width // slab):
            cut = slice(p * slab, (p + 1) * slab)
            out = raw_ref[:, cut]
            for hh in range(per):
                h = p * per + hh
                state = s_ref[h].astype(BF16)
                blank = jnp.zeros_like(state)
                if per > 1:
                    state = jnp.concatenate([state if k == hh else blank for k in range(per)], axis=0)
                out = out + dot(qd_ref[:, h * REC_KEY : (h + 1) * REC_KEY], state, ((1,), (1,)))
            square = out * out
            scale = jnp.zeros_like(out)
            for hh in range(per):
                mean = jnp.sum(jnp.where(lane == hh, square, 0.0), axis=1, keepdims=True) / REC_VAL
                scale = jnp.where(lane == hh, lax.rsqrt(mean + epsilon), scale)
            gated = g_ref[:, cut].astype(F32)
            out = out * scale * n_ref[...] * (gated * jax.nn.sigmoid(gated))
            o_ref[:, cut] = out.astype(BF16)

    vmem = pl.BlockSpec(memory_space=pltpu.VMEM)
    return pl.pallas_call(
        body,
        in_specs=[pl.BlockSpec(memory_space=pltpu.SMEM), vmem, vmem, vmem, vmem, vmem],
        out_specs=vmem,
        out_shape=jax.ShapeDtypeStruct((rows, width), BF16),
        scratch_shapes=[pltpu.VMEM((heads, REC_VAL, REC_KEY), F32)],
        name="finish_recurrence",
    )(place, raw, decayed, states, gate, jnp.tile(gain, per)[None, :])


def shards(
    tokens,
    input_norm_gain,
    attention_query_weight,
    attention_key_weight,
    attention_value_weight,
    attention_score_bias,
    recurrence_query_weight,
    forget_weight,
    input_weight,
    output_gate_weight,
    forget_minimum,
    decay_spikes,
    head_norm_gain,
    attention_output_weight,
    recurrence_output_weight,
):
    parts = lax.axis_size("tp")
    mine = lax.axis_index("tp")
    place = lax.axis_index("sp").astype(jnp.int32)[None]
    pair = parts == 2
    swap = [(0, 1), (1, 0)]
    features = tokens.shape[1]
    if pair:
        other = lax.ppermute(tokens, "tp", swap)
        full = jnp.where(
            mine == 0,
            jnp.concatenate([tokens, other], axis=1),
            jnp.concatenate([other, tokens], axis=1),
        )
        att_w, rec_w, full = lax.optimization_barrier(
            (attention_output_weight, recurrence_output_weight, full)
        )

        def half(array, which):
            return lax.dynamic_slice_in_dim(array, which * features, features, 1)

        sent_att = lax.ppermute(half(att_w, 1 - mine), "tp", swap)
        sent_rec = lax.ppermute(half(rec_w, 1 - mine), "tp", swap)
    else:
        full = lax.all_gather(tokens, "tp", axis=1, tiled=True)
    query, keys_values, rec_query, rec_forget, rec_input, rec_gate = project(
        full,
        input_norm_gain,
        (
            attention_query_weight,
            attention_key_weight,
            attention_value_weight,
            recurrence_query_weight,
            forget_weight,
            input_weight,
            output_gate_weight,
        ),
    )
    all_pairs = lax.all_gather(keys_values, "sp", axis=0, tiled=True)
    raw, decayed, state = local_recurrence(
        rec_query, rec_forget, rec_input, forget_minimum, decay_spikes
    )
    states = lax.all_gather(state, "sp")
    state_heads = finish_recurrence(place, raw, decayed, states, rec_gate, head_norm_gain)
    if pair:
        other_state = lax.ppermute(state_heads, "tp", swap)
    stick_heads = stick(place, attention_score_bias, query, all_pairs)
    if pair:
        other_stick = lax.ppermute(stick_heads, "tp", swap)
        mixed = dot(state_heads, half(rec_w, mine)) + dot(other_state, sent_rec)
        mixed = mixed + dot(stick_heads, half(att_w, mine)) + dot(other_stick, sent_att)
    else:
        stick_all = lax.all_gather(stick_heads, "tp", axis=1, tiled=True)
        state_all = lax.all_gather(state_heads, "tp", axis=1, tiled=True)
        att_cols = lax.all_to_all(
            attention_output_weight, "tp", split_axis=1, concat_axis=0, tiled=True
        )
        rec_cols = lax.all_to_all(
            recurrence_output_weight, "tp", split_axis=1, concat_axis=0, tiled=True
        )
        mixed = dot(stick_all, att_cols) + dot(state_all, rec_cols)
    return mixed.astype(BF16)


def solution(mesh):
    placed = (
        P("sp", "tp"),
        P(),
        P(None, "tp"),
        P(None, "tp"),
        P(None, "tp"),
        P("tp"),
        P(None, "tp"),
        P(None, "tp"),
        P(None, "tp"),
        P(None, "tp"),
        P("tp", None),
        P("sp", "tp"),
        P(),
        P("tp", None),
        P("tp", None),
    )
    return jax.shard_map(
        shards, mesh=mesh, in_specs=placed, out_specs=P("sp", "tp"), check_vma=False
    )
```

time: 394 us -> 171 us (0.43)
  other arithmetic: 141 us -> 2.59 us
  local copies, waits for them, and re-layouts: 68.8 us -> 3.78 us
  matrix products: 46.7 us -> 5.98 us
  Pallas kernels: 0 us -> 39.9 us
  blocking collectives: 30 us -> 0 us
  waiting for transfers between devices: 83.2 us -> 95.5 us
    another operation x16 -> x0, other arithmetic: 51.3 us -> none
    dot_general x30 -> x4, matrix products: 46.7 us -> 5.98 us  [dot(): lax.dot_general(a, b, (dims, ((), ())), precision=precision, preferred_el...]
    pallas_call x0 -> x4, Pallas kernels: none -> 39.9 us  [the longest x1 21.5 us: stick(): pl.pallas_call(body, grid=(slabs,), in_specs=[pl.BlockSpec(memory_space=p...]
    all_gather x3 -> x0, blocking collectives: 30 us -> none  [the longest x1 17.1 us: entering(): gathered = jax.tree.map(lambda a: lax.all_gather(a, axis), part)]
    dot_general x4 -> x0, other arithmetic: 29.4 us -> none  [advance(): jnp.einsum('thk,shk,tshk->hts', window_query, window_admitted, decay_tabl...]
    convert_element_type x6 -> x0, other arithmetic: 26.5 us -> none  [the longest x4 26.4 us: key_block(): weights_here = jnp.where(before, jnp.exp(jax.nn.log_sigmoid(scores) + lat...]
    while x4 -> x0, other arithmetic: 23.6 us -> none
    all_to_all x2 -> x0, waiting for transfers between devices: 21.2 us -> none  [the longest x1 12.4 us: shards(): lax.all_to_all(attention_output_weight, 'tp', split_axis=1, concat_axis=0...]
  transfers between devices with their start and end apart: 6 -> 7, of which waited for: 4 -> 5; matrix products, arithmetic and copies ran while one was open for 9% -> 4% of each run, Pallas kernels for 0% -> 15%
where the time goes in v1:
time: 171 us; the launch traced here: 168 us
  waiting for transfers between devices  95.5 us (56%)
  Pallas kernels  39.9 us (23%)
  between operations  13.5 us (8%)
  starting transfers between devices  6.56 us (4%)
  matrix products  5.98 us (3%)
  local copies, waits for them, and re-layouts  3.78 us (2%)
  other arithmetic  2.59 us (2%)
    all_gather x1, waiting for transfers between devices, shards(): all_pairs = lax.all_gather(keys_values, 'sp', axis=0, tiled=True)  40.7 us
    all_gather x1, waiting for transfers between devices, shards(): states = lax.all_gather(state, 'sp')  37.7 us
    pallas_call x1, Pallas kernels, stick(): pl.pallas_call(body, grid=(slabs,), in_specs=[pl.BlockSpec(memory_space=p...  21.5 us
    ppermute x1, waiting for transfers between devices, shards(): other = lax.ppermute(tokens, 'tp', swap)  10.9 us
    pallas_call x1, Pallas kernels, project(): pl.pallas_call(body, grid=(steps,), in_specs=[pl.BlockSpec((rows, step),...  9.83 us
    dot_general x4, matrix products, dot(): lax.dot_general(a, b, (dims, ((), ())), precision=precision, preferred_el...  5.98 us
    pallas_call x1, Pallas kernels, local_recurrence(): pl.pallas_call(body, out_shape=[jax.ShapeDtypeStruct((rows, width), F32),...  5.39 us
  transfers between devices with their start and end apart: 7, of which 5 were waited for; matrix products, arithmetic and copies ran while one was open for 4% of the time, Pallas kernels for 15%

profile of v1, /device:TPU:24, one launch (start us, length us, event | category | flops | bytes accessed | tf_op | source)
XLA Modules:
  0.0 167.8 jit_solution(6659760042752081833)
XLA Ops:
  6.5 0.0 copy-start
  6.5 0.0 all-gather.6.cloned.1.call-start
  6.5 1.5 collective-permute-start
  8.0 1.5 copy.17.s_ref
  9.5 10.9 %collective-permute-done = bf16[256,1024]{1,0:T(8,128)(2,1)S(1)} collective-permute-done((bf16[256,1024]{1,0:T(8,128)(2,1)}, bf16[256,1024]{1,0:T(8,128)(2,1)S(1)}, u32[]{:S(2)}, u32[]{:S(2)}) %collective-permute-start) | collective-permute-done | bytes 524320 | tf_op jit(solution)/shard_map/ppermute | solution.py:286
  20.4 2.6 %maximum_select_fusion.x_ref = bf16[256,2048]{1,0:T(8,128)(2,1)} fusion(bf16[256,1024]{1,0:T(8,128)(2,1)S(1)} %collective-permute-done, bf16[256,1024]{1,0:T(8,128)(2,1)} %param.15, pred[]{:T(512)S(6)} %eq.3), kind=kLoop, calls=%fused_computation.4 | loop fusion | flops 4718592 | bytes 2097153 | tf_op jit(solution)/shard_map/jit(_where)/select_n | solution.py:287
  23.0 9.8 %project.1 = (bf16[256,256]{1,0:T(8,128)(2,1)}, bf16[256,512]{1,0:T(8,128)(2,1)}, bf16[256,512]{1,0:T(8,128)(2,1)}, bf16[256,512]{1,0:T(8,128)(2,1)}, bf16[256,2...) custom-call(bf16[256,2048]{1,0:T(8,128)(2,1)} %maximum_select_fusion.x_ref, f32[1,2048]{1,0:T(1,128)} %bitcast.12, ...), custom_call_target="tpu_custom_call" | custom-call | tf_op jit(solution)/shard_map/project/pallas_call | solution.py:70
  32.8 0.0 copy-start.1
  32.9 5.4 %local_recurrence.1 = (f32[256,256]{1,0:T(8,128)}, bf16[256,512]{1,0:T(8,128)(2,1)}, f32[4,72,128]{2,1,0:T(8,128)}) custom-call(bf16[256,512]{1,0:T(8,128)(2,1)} %get-tuple-element.18.q_ref, bf16[256,512]{1,0:T(8,128)(2,1)} %get-tuple-element.19.f_ref, bf16[256,256]{1,0:T(8,128)(2,1)} %get-tuple-element.20.x_ref, f32[4,128]{1,0:T(4,128)} %m_ref.1, ...), custom_call_target="tpu_custom_call" | custom-call | tf_op jit(solution)/shard_map/local_recurrence/pallas_call | solution.py:206
  38.2 0.0 all-gather.6.cloned.1.call-update
  38.3 0.0 all-gather.4.cloned.1.call-start
  38.3 0.7 all-gather.4.cloned.1.call-update
  39.1 1.6 collective-permute-start.2
  40.6 0.6 broadcast_in_dim_tile.3.n_ref
  41.2 0.9 constant_dynamic-slice_fusion
  42.1 0.5 collective-permute-start.4
  42.6 37.7 %all-gather.6.cloned.1.call-done = f32[64,72,128]{2,1,0:T(8,128)} async-done(((f32[4,72,128]{2,1,0:T(8,128)}), f32[64,72,128]{2,1,0:T(8,128)}) %all-gather.6.cloned.1.call-update) | async-done | bytes 2359312 | tf_op jit(solution)/shard_map/all_gather | solution.py:320
  80.3 3.2 %finish_recurrence.1 = bf16[256,256]{1,0:T(8,128)(2,1)} custom-call(s32[1]{0:T(128)} %bitcast.place_ref, f32[256,256]{1,0:T(8,128)} %get-tuple-element.21.raw_ref, bf16[256,512]{1,0:T(8,128)(2,1)} %get-tuple-element.22.qd_ref, f32[16,4,72,128]{3,2,1,0:T(8,128)} %bitcast.10, bf16[256,256]{1,0:T(8,128)(2,1)} %get-tuple-element.24.g_ref, ...), custom_call_target="tpu_custom_call" | custom-call | tf_op jit(solution)/shard_map/finish_recurrence/pallas_call | solution.py:252
  83.5 1.5 collective-permute-start.1
  85.0 1.2 fusion.2
  86.2 0.0 collective-permute-done.2
  86.2 0.0 copy-start.2
  86.2 0.8 copy-done.2
  87.0 2.3 %collective-permute-done.1 = bf16[256,256]{1,0:T(8,128)(2,1)S(1)} collective-permute-done((bf16[256,256]{1,0:T(8,128)(2,1)}, bf16[256,256]{1,0:T(8,128)(2,1)S(1)}, u32[]{:S(2)}, u32[]{:S(2)}) %collective-permute-start.1) | collective-permute-done | bytes 131104 | tf_op jit(solution)/shard_map/ppermute | solution.py:323
  89.4 1.4 convolution_add_fusion.2
  90.7 40.7 %all-gather.4.cloned.1.call-done.k_ref.v_ref = bf16[4096,512]{1,0:T(8,128)(2,1)} async-done(((bf16[256,512]{1,0:T(8,128)(2,1)}), bf16[4096,512]{1,0:T(8,128)(2,1)}) %all-gather.4.cloned.1.call-update) | async-done | bytes 4194320 | tf_op jit(solution)/shard_map/all_gather | solution.py:316
  131.4 21.5 %stick.1 = bf16[256,256]{1,0:T(8,128)(2,1)} custom-call(s32[1]{0:T(128)} %bitcast.place_ref, f32[4]{0:T(128)} %bias_ref.1, bf16[256,256]{1,0:T(8,128)(2,1)} %get-tuple-element.26.q_ref, bf16[4096,512]{1,0:T(8,128)(2,1)} %all-gather.4.cloned.1.call-done.k_ref.v_ref, bf16[4096,512]{1,0:T(8,128)(2,1)} %all-gather.4.cloned.1.call-done.k_ref.v_ref), custom_call_target="tpu_custom_call" | custom-call | tf_op jit(solution)/shard_map/stick/pallas_call | solution.py:140
  153.0 1.5 collective-permute-start.3
  154.5 1.2 convolution_add_fusion.1
  155.7 0.0 collective-permute-done.4
  155.7 3.1 %collective-permute-done.3 = bf16[256,256]{1,0:T(8,128)(2,1)S(1)} collective-permute-done((bf16[256,256]{1,0:T(8,128)(2,1)}, bf16[256,256]{1,0:T(8,128)(2,1)S(1)}, u32[]{:S(2)}, u32[]{:S(2)}) %collective-permute-start.3) | collective-permute-done | bytes 131104 | tf_op jit(solution)/shard_map/ppermute | solution.py:326
  158.8 2.1 %fusion = bf16[256,1024]{1,0:T(8,128)(2,1)} fusion(f32[256,1024]{1,0:T(8,128)S(1)} %convolution_add_fusion.1, bf16[256,256]{1,0:T(8,128)(2,1)S(1)} %collective-permute-done.3, bf16[256,1024]{1,0:T(8,128)(2,1)} %collective-permute-done.4), kind=kOutput, calls=%fused_computation.3 | convolution fusion | flops 134742016 | bytes 2228224 | tf_op jit(solution)/shard_map/dot_general | solution.py:20
  (6 shorter events, 0.1 us)
Async XLA Ops:
  6.5 32.5 %copy-start = (bf16[256,2048]{1,0:T(8,128)(2,1)S(1)}, bf16[256,2048]{1,0:T(8,128)(2,1)}, u32[]{:S(2)}) copy-start(bf16[256,2048]{1,0:T(8,128)(2,1)} %param.29) | copy-start | bytes 3145732
  6.5 73.8 %all-gather.6.cloned.1.call-start = ((), (), s32[]{:S(2)}) async-start(), calls=%async_computation.1 | async-start | bytes 2506752 | tf_op jit(solution)/shard_map/all_gather | solution.py:320
  6.5 13.9 %collective-permute-start = (bf16[256,1024]{1,0:T(8,128)(2,1)}, bf16[256,1024]{1,0:T(8,128)(2,1)S(1)}, u32[]{:S(2)}, u32[]{:S(2)}) collective-permute-start(bf16[256,1024]{1,0:T(8,128)(2,1)} %param.15), channel_id=1, source_target_pairs={{0,1},{1,0},{2,3},{3,2},{4,5},{5,4},{6,7},{7,6},{8,9},{9,8},{10,11... | collective-permute-start | bytes 1572872 | tf_op jit(solution)/shard_map/ppermute | solution.py:286
  32.8 7.8 %copy-start.3 = (f32[64]{0:T(128)S(1)}, f32[64]{0:T(128)}, u32[]{:S(2)}) copy-start(f32[64]{0:T(128)} %param.27) | copy-start | bytes 772
  32.8 8.4 %copy-start.1 = (bf16[256,2048]{1,0:T(8,128)(2,1)S(1)}, bf16[256,2048]{1,0:T(8,128)(2,1)}, u32[]{:S(2)}) copy-start(bf16[256,2048]{1,0:T(8,128)(2,1)} %param.28) | copy-start | bytes 3145732
  38.3 93.2 %all-gather.4.cloned.1.call-start = ((), (), s32[]{:S(2)}) async-start(), calls=%async_computation | async-start | bytes 4456448 | tf_op jit(solution)/shard_map/all_gather | solution.py:316
  39.1 47.1 %collective-permute-start.2 = (bf16[256,1024]{1,0:T(8,128)(2,1)S(1)}, bf16[256,1024]{1,0:T(8,128)(2,1)S(1)}, u32[]{:S(2)}, u32[]{:S(2)}) collective-permute-start(bf16[256,1024]{1,0:T(8,128)(2,1)S(1)} %constant_dynamic-slice_fusion.1), channel_id=1, source_target_pairs={{0,1},{1,0},{2,3},{3,2},{4,5},{5,4},{6,7},{7,6},{8,9},{9,8},{10,11... | collective-permute-start | bytes 1572872 | tf_op jit(solution)/shard_map/ppermute | solution.py:300
  42.1 113.6 %collective-permute-start.4 = (bf16[256,1024]{1,0:T(8,128)(2,1)}, bf16[256,1024]{1,0:T(8,128)(2,1)}, u32[]{:S(2)}, u32[]{:S(2)}) collective-permute-start(bf16[256,1024]{1,0:T(8,128)(2,1)} %constant_dynamic-slice_fusion), channel_id=1, source_target_pairs={{0,1},{1,0},{2,3},{3,2},{4,5},{5,4},{6,7},{7,6},{8,9},{9,8},{10,11... | collective-permute-start | bytes 1572872 | tf_op jit(solution)/shard_map/ppermute | solution.py:299
  83.5 5.9 %collective-permute-start.1 = (bf16[256,256]{1,0:T(8,128)(2,1)}, bf16[256,256]{1,0:T(8,128)(2,1)S(1)}, u32[]{:S(2)}, u32[]{:S(2)}) collective-permute-start(bf16[256,256]{1,0:T(8,128)(2,1)} %finish_recurrence.1), channel_id=1, source_target_pairs={{0,1},{1,0},{2,3},{3,2},{4,5},{5,4},{6,7},{7,6},{8,9},{9,8},{10,11... | collective-permute-start | bytes 393224 | tf_op jit(solution)/shard_map/ppermute | solution.py:323
  86.2 0.8 copy-start.2
  153.0 5.8 %collective-permute-start.3 = (bf16[256,256]{1,0:T(8,128)(2,1)}, bf16[256,256]{1,0:T(8,128)(2,1)S(1)}, u32[]{:S(2)}, u32[]{:S(2)}) collective-permute-start(bf16[256,256]{1,0:T(8,128)(2,1)} %stick.1), channel_id=1, source_target_pairs={{0,1},{1,0},{2,3},{3,2},{4,5},{5,4},{6,7},{7,6},{8,9},{9,8},{10,11... | collective-permute-start | bytes 393224 | tf_op jit(solution)/shard_map/ppermute | solution.py:326
Sparse Core Ops, SparseCore 0:
  38.4 41.9 all-gather.5
  82.5 48.8 all-gather.3
